TPU v7x, 32 devices: a whole 2x2x4 slice. The times are simulated.
32 devices in a mesh: ep: 4 (over z), tp: 8 (over y, x, core).
Axes of the slice: x: 2, y: 2, z: 4, core: 2. Of those that a mesh axis runs over, the one named last changes fastest.
Arguments:
- tokens: bfloat16 [32, 4096], P('ep'), may hold values from -6 to 6
- norm_gains: float32 [4, 4096], replicated, may hold values from 0.1 to 1.9
- w_query: bfloat16 [4096, 4096], P(None, 'tp'), may hold values from -0.09375 to 0.09375
- w_query_rope: bfloat16 [4096, 2048], P(None, 'tp'), may hold values from -0.09375 to 0.09375
- w_key_up: bfloat16 [32, 128, 1024], P('tp'), may hold values from -0.5 to 0.5
- w_value_up: bfloat16 [32, 1024, 128], P('tp'), may hold values from -0.1875 to 0.1875
- w_output: bfloat16 [4096, 4096], P('tp'), may hold values from -0.09375 to 0.09375
- w_latent_down: bfloat16 [4096, 1024], P(None, 'tp'), may hold values from -0.09375 to 0.09375
- latent_gain: float32 [1024], replicated, may hold values from 0.1 to 1.9
- w_rope_down: bfloat16 [4096, 64], replicated, may hold values from -0.09375 to 0.09375
- cache_latent: bfloat16 [32, 1024, 1024], P(('ep', 'tp')), may hold values from -300 to 300
- cache_rope: bfloat16 [32, 1024, 64], P(('ep', 'tp')), may hold values from -6 to 6
- lengths: int32 [32], P(('ep', 'tp')), may hold values from 1 to 1024, as said below
- routes: int32 [32, 2], P('ep'), may hold values from 0 to 3, all different within a row; in each aligned block of 8 rows (0 to 7, 8 to 15, ...) at most 7 rows name the same one
- route_weights: float32 [32, 2], P('ep'), may hold values from 0.2 to 1
- w_gate: bfloat16 [4, 4096, 2048], P('ep', None, 'tp'), may hold values from -0.09375 to 0.09375
- w_up: bfloat16 [4, 4096, 2048], P('ep', None, 'tp'), may hold values from -0.09375 to 0.09375
- w_down: bfloat16 [4, 2048, 4096], P('ep', 'tp'), may hold values from -0.125 to 0.125
Outputs:
- hidden_out: bfloat16 [32, 4096], P(('ep', 'tp'))
- new_latent: bfloat16 [32, 1024], P(('ep', 'tp'))
- new_rope: bfloat16 [32, 64], P(('ep', 'tp'))
Inputs may be any that keep to these rules, and one draw needn't show every extreme that they name: `routes`: within each aligned block of 8 rows no expert is named by more than 7 rows, a bound that some block reaches; the 2 experts of a row differ. The new token stands at position lengths; some sequence has exactly 1024.
All inputs are finite; a program needn't handle non-finite values.
Results may differ from a plain program's by a relative error of at most 0.02.
Values may be sent and summed in bfloat16 or wider, within the bound.
No kernel may reach another device: no remote copies, remote signals or barrier semaphores. Data moves between devices by JAX's collectives and lax.ppermute only.
A program may use at most 64 MiB of HBM per device.

v0:
```python
import jax
import jax.numpy as jnp
from jax import lax
from jax.sharding import PartitionSpec as P

EXP_LOCAL = 1


EPSILON = 1e-06
ROTARY_BASE = 500000.0


def rms_scale(source, gain_row):
    values_f = source.astype(jnp.float32)
    return (
        values_f
        * lax.rsqrt(jnp.mean(values_f * values_f, axis=-1, keepdims=True) + EPSILON)
        * gain_row
    )


def rotate(source, position):
    half_width = source.shape[-1] // 2
    frequency = ROTARY_BASE ** (-jnp.arange(half_width, dtype=jnp.float32) / half_width)
    angles = position[..., None] * frequency
    first_half = source[..., :half_width]
    second_half = source[..., half_width:]
    return jnp.concatenate(
        [
            first_half * jnp.cos(angles) - second_half * jnp.sin(angles),
            second_half * jnp.cos(angles) + first_half * jnp.sin(angles),
        ],
        axis=-1,
    )


def attend(q_latent, q_pe, cache_lat, cache_rp, lat_new, rope_new, lengths, score_scale):
    scores = (
        jnp.einsum("shc,spc->shp", q_latent, cache_lat, preferred_element_type=jnp.float32)
        + jnp.einsum("shr,spr->shp", q_pe, cache_rp, preferred_element_type=jnp.float32)
    ) * score_scale
    own_score = (
        jnp.einsum("shc,sc->sh", q_latent, lat_new, preferred_element_type=jnp.float32)
        + jnp.einsum("shr,sr->sh", q_pe, rope_new, preferred_element_type=jnp.float32)
    ) * score_scale
    visible = (
        jnp.arange(cache_lat.shape[1], dtype=jnp.int32)[None, None, :] < lengths[:, None, None]
    )
    row_max = jnp.maximum(jnp.max(jnp.where(visible, scores, -jnp.inf), axis=-1), own_score)
    weights = jnp.where(visible, jnp.exp(scores - row_max[..., None]), 0.0)
    own_weight = jnp.exp(own_score - row_max)
    denominator = jnp.sum(weights, axis=-1) + own_weight
    probabilities = (weights / denominator[..., None]).astype(jnp.bfloat16)
    own_prob = (own_weight / denominator).astype(jnp.bfloat16)
    attended = jnp.einsum(
        "shp,spc->shc", probabilities, cache_lat, preferred_element_type=jnp.float32
    )
    attended = (
        attended + own_prob.astype(jnp.float32)[..., None] * lat_new.astype(jnp.float32)[:, None, :]
    )
    return attended.astype(jnp.bfloat16)


def on_device(
    tokens,
    norm_gains,
    w_query,
    w_query_rope,
    w_key_up,
    w_value_up,
    w_output,
    w_latent_down,
    latent_gain,
    w_rope_down,
    cache_latent,
    cache_rope,
    lengths,
    routes,
    route_weights,
    w_gate,
    w_up,
    w_down,
):
    group_rows = tokens.shape[0]
    seq_count = cache_latent.shape[0]
    heads_here = w_key_up.shape[0]
    nope_width = w_key_up.shape[1]
    rope_width = w_rope_down.shape[1]
    tp_size = lax.axis_size("tp")
    tp_rank = lax.axis_index("tp")
    normed = rms_scale(tokens, norm_gains[0]).astype(jnp.bfloat16)
    q_nope = jnp.dot(normed, w_query, preferred_element_type=jnp.float32).astype(jnp.bfloat16)
    q_nope = q_nope.reshape(group_rows, heads_here, nope_width)
    q_latent = jnp.einsum("thn,hnc->thc", q_nope, w_key_up, preferred_element_type=jnp.float32)
    q_latent = q_latent.astype(jnp.bfloat16).reshape(group_rows, -1)
    q_rot = jnp.dot(normed, w_query_rope, preferred_element_type=jnp.float32).astype(jnp.bfloat16)
    latent_cols = jnp.dot(normed, w_latent_down, preferred_element_type=jnp.float32).astype(
        jnp.bfloat16
    )
    q_mine, rot_mine, latent_raw = (
        lax.all_to_all(q_latent, "tp", split_axis=0, concat_axis=1, tiled=True),
        lax.all_to_all(q_rot, "tp", split_axis=0, concat_axis=1, tiled=True),
        lax.all_to_all(latent_cols, "tp", split_axis=0, concat_axis=1, tiled=True),
    )
    heads_all = rot_mine.shape[1] // rope_width
    own_normed = lax.dynamic_slice_in_dim(normed, tp_rank * seq_count, seq_count, 0)
    rope_raw = jnp.dot(own_normed, w_rope_down, preferred_element_type=jnp.float32).astype(
        jnp.bfloat16
    )
    new_latent = rms_scale(latent_raw, latent_gain).astype(jnp.bfloat16)
    position = lengths.astype(jnp.float32)
    new_rope = rotate(rope_raw.astype(jnp.float32), position).astype(jnp.bfloat16)
    q_pe = rotate(
        rot_mine.reshape(seq_count, heads_all, rope_width).astype(jnp.float32), position[:, None]
    )
    q_pe = q_pe.astype(jnp.bfloat16)
    score_scale = (nope_width + rope_width) ** (-0.5)
    attended = attend(
        q_mine.reshape(seq_count, heads_all, -1),
        q_pe,
        cache_latent,
        cache_rope,
        new_latent,
        new_rope,
        lengths,
        score_scale,
    )
    head_latent = lax.all_to_all(
        attended.reshape(seq_count, -1), "tp", split_axis=1, concat_axis=0, tiled=True
    )
    values = (
        jnp.einsum(
            "thc,hcv->thv",
            head_latent.reshape(group_rows, heads_here, -1),
            w_value_up,
            preferred_element_type=jnp.float32,
        )
        .astype(jnp.bfloat16)
        .reshape(group_rows, -1)
    )
    head_term = jnp.dot(values, w_output, preferred_element_type=jnp.float32)
    mixed = lax.psum(head_term.astype(jnp.bfloat16), "tp").astype(jnp.float32)
    resid = (tokens.astype(jnp.float32) + rms_scale(mixed, norm_gains[1])).astype(jnp.bfloat16)
    expert_in = rms_scale(resid, norm_gains[2]).astype(jnp.bfloat16)
    own_resid = lax.dynamic_slice_in_dim(resid, tp_rank * seq_count, seq_count, 0)
    ep_size = lax.axis_size("ep")
    experts = ep_size * EXP_LOCAL
    local_expert = tp_rank // (tp_size // EXP_LOCAL)
    route_count = routes.shape[1]
    capacity = (
        (group_rows * route_count + experts - 1) // experts
        + 2
        + group_rows * route_count // (4 * experts)
    )
    slot_count = ep_size * capacity
    flat_routes = routes.reshape(-1)
    expert_hits = (flat_routes[:, None] == jnp.arange(experts, dtype=jnp.int32)[None, :]).astype(
        jnp.int32
    )
    slot_rank = jnp.sum((jnp.cumsum(expert_hits, axis=0) - 1) * expert_hits, axis=1)
    served_here = flat_routes % EXP_LOCAL == local_expert
    slot_index = jnp.where(served_here, flat_routes // EXP_LOCAL * capacity + slot_rank, -1)
    slot_picks = (slot_index[:, None] == jnp.arange(slot_count, dtype=jnp.int32)[None, :]).astype(
        jnp.bfloat16
    )
    slot_picks = slot_picks.reshape(group_rows, route_count, slot_count)
    slot_rows = jnp.sum(slot_picks, axis=1)
    outgoing = jnp.dot(slot_rows.T, expert_in, preferred_element_type=jnp.float32).astype(
        jnp.bfloat16
    )
    arrived = lax.all_to_all(outgoing, "ep", split_axis=0, concat_axis=0, tiled=True)
    gate_sum = jnp.dot(arrived, w_gate[0], preferred_element_type=jnp.float32)
    up_sum = jnp.dot(arrived, w_up[0], preferred_element_type=jnp.float32)
    hidden_units = (jax.nn.silu(gate_sum) * up_sum).astype(jnp.bfloat16)
    expert_out = jnp.dot(hidden_units, w_down[0], preferred_element_type=jnp.float32).astype(
        jnp.bfloat16
    )
    returned = lax.all_to_all(expert_out, "ep", split_axis=0, concat_axis=0, tiled=True)
    routed_part = jnp.zeros((group_rows, returned.shape[1]), jnp.float32)
    for route_slot in range(route_count):
        chosen = jnp.dot(slot_picks[:, route_slot, :], returned, preferred_element_type=jnp.float32)
        routed_part = routed_part + route_weights[:, route_slot : route_slot + 1] * chosen
    routed = lax.psum_scatter(
        routed_part.astype(jnp.bfloat16), "tp", scatter_dimension=0, tiled=True
    ).astype(jnp.float32)
    hidden_out = (own_resid.astype(jnp.float32) + rms_scale(routed, norm_gains[3])).astype(
        jnp.bfloat16
    )
    return (hidden_out, new_latent, new_rope)


def solution(mesh):
    in_specs = (
        P("ep", None),
        P(),
        P(None, "tp"),
        P(None, "tp"),
        P("tp", None, None),
        P("tp", None, None),
        P("tp", None),
        P(None, "tp"),
        P(),
        P(),
        P(("ep", "tp"), None, None),
        P(("ep", "tp"), None, None),
        P(("ep", "tp")),
        P("ep", None),
        P("ep", None),
        P("ep", None, "tp"),
        P("ep", None, "tp"),
        P("ep", "tp", None),
    )
    out_specs = (P(("ep", "tp"), None), P(("ep", "tp"), None), P(("ep", "tp"), None))
    return jax.shard_map(
        on_device, mesh=mesh, in_specs=in_specs, out_specs=out_specs, check_vma=False
    )
```

profile of v0, /device:TPU:0, one launch (start us, length us, event | category | flops | bytes accessed | tf_op | source)
XLA Modules:
  0.0 212.2 jit_solution(539098069489857588)
XLA Ops:
  7.2 1.1 fusion.78
  8.3 1.0 fusion.40
  9.3 0.9 fusion.42
  10.2 1.5 fusion.29
  12.3 5.2 %all-to-all-start.2 = ((bf16[8,1,128]{2,1,0:T(2,128)(2,1)}), bf16[8,1,128]{2,1,0:T(2,128)(2,1)S(1)}, u32[]{:S(2)}, u32[]{:S(2)}) async-start(bf16[8,1,128]{2,1,0:T(2,128)(2,1)} %copy.35), calls=%async_computation.2 | async-start | bytes 8192 | tf_op jit(solution)/shard_map/all_to_all | solution.py:103
  17.5 2.0 fusion.28
  20.2 1.3 fusion.34
  22.1 3.1 %convolution_convert_fusion.3 = bf16[4,8,1024]{2,1,0:T(8,128)(2,1)S(1)} fusion(bf16[4,128,1024]{2,1,0:T(8,128)(2,1)S(1)} %copy-done.2, bf16[8,4096]{1,0:T(8,128)(2,1)S(1)} %fusion.42, bf16[4096,512]{1,0:T(8,128)(2,1)} %param.20), kind=kOutput, calls=%fused_computation.20 | convolution fusion | flops 41979904 | bytes 5373952 | tf_op jit(solution)/shard_map/thn,hnc->thc/dot_general | solution.py:94
  26.9 0.7 reduce.12
  27.6 0.7 reshape.353
  28.3 4.2 %all-to-all-start.1 = ((bf16[8,2,128]{2,1,0:T(2,128)(2,1)}), bf16[8,2,128]{2,1,0:T(2,128)(2,1)S(1)}, u32[]{:S(2)}, u32[]{:S(2)}) async-start(bf16[8,2,128]{2,1,0:T(2,128)(2,1)} %reshape.355), calls=%async_computation.1 | async-start | bytes 8192 | tf_op jit(solution)/shard_map/all_to_all | solution.py:102
  33.9 3.3 %all-to-all-done.1 = bf16[8,2,128]{2,1,0:T(2,128)(2,1)S(1)} async-done(((bf16[8,2,128]{2,1,0:T(2,128)(2,1)}), bf16[8,2,128]{2,1,0:T(2,128)(2,1)S(1)}, u32[]{:S(2)}, u32[]{:S(2)}) %all-to-all-start.1) | async-done | bytes 4128 | tf_op jit(solution)/shard_map/all_to_all | solution.py:102
  37.1 3.3 %all-to-all-start = ((bf16[8,2,2048]{2,1,0:T(2,128)(2,1)}), bf16[8,2,2048]{2,1,0:T(2,128)(2,1)S(1)}, u32[]{:S(2)}, u32[]{:S(2)}) async-start(bf16[8,2,2048]{2,1,0:T(2,128)(2,1)} %reshape.353), calls=%async_computation | async-start | bytes 131072 | tf_op jit(solution)/shard_map/all_to_all | solution.py:101
  40.7 4.8 %all-to-all-done = bf16[8,2,2048]{2,1,0:T(2,128)(2,1)S(1)} async-done(((bf16[8,2,2048]{2,1,0:T(2,128)(2,1)}), bf16[8,2,2048]{2,1,0:T(2,128)(2,1)S(1)}, u32[]{:S(2)}, u32[]{:S(2)}) %all-to-all-start) | async-done | bytes 65568 | tf_op jit(solution)/shard_map/all_to_all | solution.py:101
  46.0 2.5 %fusion.9 = f32[32,1024]{1,0:T(8,128)S(1)} fusion(bf16[32,1024]{1,0:T(8,128)(2,1)S(1)} %reshape.334, bf16[1,1024,1024]{2,1,0:T(8,128)(2,1)} %param.28), kind=kOutput, calls=%fused_computation.14 | convolution fusion | flops 67108864 | bytes 2293760 | tf_op jit(solution)/shard_map/shc,spc->shp/dot_general | solution.py:39
  49.9 1.0 reduce.14
  51.6 3.3 %all-to-all-start.3 = ((bf16[8,2,2048]{2,1,0:T(2,128)(2,1)}), bf16[8,2,2048]{2,1,0:T(2,128)(2,1)S(1)}, u32[]{:S(2)}, u32[]{:S(2)}) async-start(bf16[8,2,2048]{2,1,0:T(2,128)(2,1)} %reshape.357), calls=%async_computation.3 | async-start | bytes 131072 | tf_op jit(solution)/shard_map/all_to_all | solution.py:128
  55.1 4.8 %all-to-all-done.3 = bf16[8,2,2048]{2,1,0:T(2,128)(2,1)S(1)} async-done(((bf16[8,2,2048]{2,1,0:T(2,128)(2,1)}), bf16[8,2,2048]{2,1,0:T(2,128)(2,1)S(1)}, u32[]{:S(2)}, u32[]{:S(2)}) %all-to-all-start.3) | async-done | bytes 65568 | tf_op jit(solution)/shard_map/all_to_all | solution.py:128
  60.3 3.7 %convolution_convert_fusion.2 = bf16[8,4096]{1,0:T(8,128)(2,1)} fusion(bf16[512,4096]{1,0:T(8,128)(2,1)} %param.24, bf16[8,4,1024]{2,0,1:T(8,128)(2,1)S(1)} %bitcast.123, bf16[4,1024,128]{2,1,0:T(8,128)(2,1)S(1)} %copy-done.3), kind=kOutput, calls=%fused_computation.6 | convolution fusion | flops 41979904 | bytes 5373952 | tf_op jit(solution)/shard_map/dot_general | solution.py:141
  64.1 52.6 %all-reduce.4.cloned.1.call-done = bf16[8,4096]{1,0:T(8,128)(2,1)} async-done(((bf16[8,4096]{1,0:T(8,128)(2,1)}), bf16[8,4096]{1,0:T(8,128)(2,1)}) %all-reduce.4.cloned.1.call-update) | async-done | bytes 65552 | tf_op jit(solution)/shard_map/psum | solution.py:142
  116.7 1.0 fusion.35
  117.7 1.1 fusion.37
  119.2 12.5 %all_to_all.77 = bf16[4,7,4096]{2,1,0:T(8,128)(2,1)S(1)} all-to-all(bf16[4,7,4096]{2,1,0:T(8,128)(2,1)S(1)} %all_to_all.64), channel_id=1, replica_groups=mesh['ep'=4,'tp'=8] {'ep'}, dimensions={0} | all-to-all | bytes 458752 | tf_op jit(solution)/shard_map/all_to_all | solution.py:171
  131.8 2.1 fusion.5
  133.9 2.9 %convolution_convert_fusion = bf16[28,4096]{1,0:T(8,128)(2,1)S(1)} fusion(bf16[1,256,4096]{2,1,0:T(8,128)(2,1)S(1)} %copy-done, bf16[28,4096]{1,0:T(8,128)(2,1)S(1)} %all_to_all.66, bf16[1,4096,256]{2,1,0:T(8,128)(2,1)} %param.34, f32[28,256]{1,0:T(8,128)S(1)} %fusion.5), kind=kOutput, calls=%fused_computation | convolution fusion | flops 117598208 | bytes 4681728 | tf_op jit(solution)/shard_map/dot_general | solution.py:175
  136.7 0.8 all_to_all.67
  137.5 3.4 %all-to-all-start.5 = ((bf16[4,7,4096]{2,1,0:T(8,128)(2,1)}), bf16[4,7,4096]{2,1,0:T(8,128)(2,1)S(1)}, u32[]{:S(2)}, u32[]{:S(2)}) async-start(bf16[4,7,4096]{2,1,0:T(8,128)(2,1)} %all_to_all.67), calls=%async_computation.5 | async-start | bytes 524288 | tf_op jit(solution)/shard_map/all_to_all | solution.py:178
  141.1 7.7 %all-to-all-done.5 = bf16[4,7,4096]{2,1,0:T(8,128)(2,1)S(1)} async-done(((bf16[4,7,4096]{2,1,0:T(8,128)(2,1)}), bf16[4,7,4096]{2,1,0:T(8,128)(2,1)S(1)}, u32[]{:S(2)}, u32[]{:S(2)}) %all-to-all-start.5) | async-done | bytes 229408 | tf_op jit(solution)/shard_map/all_to_all | solution.py:178
  149.1 0.8 fusion.1
  151.6 48.9 %all-reduce.6.cloned.1.call-done = bf16[8,4096]{1,0:T(8,128)(2,1)} async-done(((bf16[8,4096]{1,0:T(8,128)(2,1)}), bf16[8,4096]{1,0:T(8,128)(2,1)}) %all-reduce.6.cloned.1.call-update) | async-done | bytes 65552
  200.5 2.0 multiply_reduce_fusion
  203.2 2.1 add_convert_fusion
  (75 shorter events, 9.8 us)
Async XLA Ops:
  7.2 126.7 %copy-start = (bf16[1,256,4096]{2,1,0:T(8,128)(2,1)S(1)}, bf16[1,256,4096]{2,1,0:T(8,128)(2,1)}, u32[]{:S(2)}) copy-start(bf16[1,256,4096]{2,1,0:T(8,128)(2,1)} %param.35) | copy-start | bytes 6291460
  7.2 14.4 %copy-start.7 = (s32[8,2]{0,1:T(2,128)S(1)}, s32[8,2]{0,1:T(2,128)}, u32[]{:S(2)}) copy-start(s32[8,2]{0,1:T(2,128)} %param.31) | copy-start | bytes 196
  7.2 14.8 %copy-start.2 = (bf16[4,128,1024]{2,1,0:T(8,128)(2,1)S(1)}, bf16[4,128,1024]{2,1,0:T(8,128)(2,1)}, u32[]{:S(2)}) copy-start(bf16[4,128,1024]{2,1,0:T(8,128)(2,1)} %param.22) | copy-start | bytes 3145732
  12.3 16.0 %all-to-all-start.2 = ((bf16[8,1,128]{2,1,0:T(2,128)(2,1)}), bf16[8,1,128]{2,1,0:T(2,128)(2,1)S(1)}, u32[]{:S(2)}, u32[]{:S(2)}) async-start(bf16[8,1,128]{2,1,0:T(2,128)(2,1)} %copy.35), calls=%async_computation.2 | async-start | bytes 8192 | tf_op jit(solution)/shard_map/all_to_all | solution.py:103
  22.0 11.8 %copy-start.6 = (f32[1024]{0:T(1024)S(1)}, f32[1024]{0:T(1024)}, u32[]{:S(2)}) copy-start(f32[1024]{0:T(1024)} %param.26) | copy-start | bytes 12292
  25.1 23.4 %copy-start.5 = (bf16[1,1024,64]{1,2,0:T(8,128)(2,1)S(1)}, bf16[1,1024,64]{1,2,0:T(8,128)(2,1)}, u32[]{:S(2)}) copy-start(bf16[1,1024,64]{1,2,0:T(8,128)(2,1)} %param.29) | copy-start | bytes 393220
  28.3 8.8 %all-to-all-start.1 = ((bf16[8,2,128]{2,1,0:T(2,128)(2,1)}), bf16[8,2,128]{2,1,0:T(2,128)(2,1)S(1)}, u32[]{:S(2)}, u32[]{:S(2)}) async-start(bf16[8,2,128]{2,1,0:T(2,128)(2,1)} %reshape.355), calls=%async_computation.1 | async-start | bytes 8192 | tf_op jit(solution)/shard_map/all_to_all | solution.py:102
  37.1 8.3 %all-to-all-start = ((bf16[8,2,2048]{2,1,0:T(2,128)(2,1)}), bf16[8,2,2048]{2,1,0:T(2,128)(2,1)S(1)}, u32[]{:S(2)}, u32[]{:S(2)}) async-start(bf16[8,2,2048]{2,1,0:T(2,128)(2,1)} %reshape.353), calls=%async_computation | async-start | bytes 131072 | tf_op jit(solution)/shard_map/all_to_all | solution.py:101
  45.9 3.4 %copy-start.1 = (bf16[1,1024,1024]{2,1,0:T(8,128)(2,1)S(1)}, bf16[1,1024,1024]{2,1,0:T(8,128)(2,1)}, u32[]{:S(2)}) copy-start(bf16[1,1024,1024]{2,1,0:T(8,128)(2,1)} %param.28) | copy-start | bytes 6291460
  48.4 11.9 %copy-start.3 = (bf16[4,1024,128]{2,1,0:T(8,128)(2,1)S(1)}, bf16[4,1024,128]{2,1,0:T(8,128)(2,1)}, u32[]{:S(2)}) copy-start(bf16[4,1024,128]{2,1,0:T(8,128)(2,1)} %param.23) | copy-start | bytes 3145732
  51.6 8.3 %all-to-all-start.3 = ((bf16[8,2,2048]{2,1,0:T(2,128)(2,1)}), bf16[8,2,2048]{2,1,0:T(2,128)(2,1)S(1)}, u32[]{:S(2)}, u32[]{:S(2)}) async-start(bf16[8,2,2048]{2,1,0:T(2,128)(2,1)} %reshape.357), calls=%async_computation.3 | async-start | bytes 131072 | tf_op jit(solution)/shard_map/all_to_all | solution.py:128
  54.9 61.8 %all-reduce.4.cloned.1.call-start = ((), (), s32[]{:S(2)}) async-start(), calls=%async_computation.6 | async-start | bytes 131072 | tf_op jit(solution)/shard_map/psum | solution.py:142
  60.3 57.4 %copy-start.4 = (bf16[8,4096]{1,0:T(8,128)(2,1)S(1)}, bf16[8,4096]{1,0:T(8,128)(2,1)}, u32[]{:S(2)}) copy-start(bf16[8,4096]{1,0:T(8,128)(2,1)} %param.18) | copy-start | bytes 196612
  133.8 7.1 %copy-start.8 = (f32[8,2]{0,1:T(2,128)S(1)}, f32[8,2]{0,1:T(2,128)}, u32[]{:S(2)}) copy-start(f32[8,2]{0,1:T(2,128)} %param.32) | copy-start | bytes 196
  136.7 13.7 %copy-start.9 = (u32[32]{0:T(128)S(1)}, u32[32]{0:T(128)}, u32[]{:S(2)}) copy-start(u32[32]{0:T(128)} %constant.96) | copy-start | bytes 388
  137.5 11.3 %all-to-all-start.5 = ((bf16[4,7,4096]{2,1,0:T(8,128)(2,1)}), bf16[4,7,4096]{2,1,0:T(8,128)(2,1)S(1)}, u32[]{:S(2)}, u32[]{:S(2)}) async-start(bf16[4,7,4096]{2,1,0:T(8,128)(2,1)} %all_to_all.67), calls=%async_computation.5 | async-start | bytes 524288 | tf_op jit(solution)/shard_map/all_to_all | solution.py:178
  140.9 59.6 %all-reduce.6.cloned.1.call-start = ((), (), s32[]{:S(2)}) async-start(), calls=%async_computation.7 | async-start | bytes 131072
Sparse Core Ops, SparseCore 0:
  64.2 52.5 all-reduce.3
  150.0 50.4 all-reduce.5
where the time goes:
time: 213 us; the launch traced here: 212 us
  waiting for transfers between devices  122 us (57%)
  matrix products  21.2 us (10%)
  starting transfers between devices  19.6 us (9%)
  between operations  16.4 us (8%)
  other arithmetic  12.9 us (6%)
  blocking collectives  12.5 us (6%)
  local copies, waits for them, and re-layouts  7.42 us (3%)
    psum x1, waiting for transfers between devices, on_device(): mixed = lax.psum(head_term.astype(jnp.bfloat16), 'tp').astype(jnp.float32)  52.6 us
    unnamed x3, waiting for transfers between devices  48.9 us
    all_to_all x1, blocking collectives, on_device(): lax.all_to_all(outgoing, 'ep', split_axis=0, concat_axis=0, tiled=True)  12.5 us
    all_to_all x1, waiting for transfers between devices, on_device(): lax.all_to_all(expert_out, 'ep', split_axis=0, concat_axis=0, tiled=True)  7.75 us
    reduce_sum x5, other arithmetic, rms_scale(): jnp.mean(values_f * values_f, axis=-1, keepdims=True) + EPSILON  5.68 us
    all_to_all x1, starting transfers between devices, on_device(): lax.all_to_all(latent_cols, 'tp', split_axis=0, concat_axis=1, tiled=True)  5.2 us
    all_to_all x1, waiting for transfers between devices, on_device(): lax.all_to_all(attended.reshape(seq_count, -1), 'tp', split_axis=1, conca...  4.81 us
    all_to_all x1, waiting for transfers between devices, on_device(): lax.all_to_all(q_latent, 'tp', split_axis=0, concat_axis=1, tiled=True)  4.75 us
  transfers between devices with their start and end apart: 7, of which 6 were waited for; matrix products, arithmetic and copies ran while one was open for 6% of the time, Pallas kernels for 0%

commit v1 on v0

--- a/solution.py
+++ b/solution.py
@@ -2,9 +2,6 @@
 import jax.numpy as jnp
 from jax import lax
 from jax.sharding import PartitionSpec as P
-
-EXP_LOCAL = 1
-
 
 EPSILON = 1e-06
 ROTARY_BASE = 500000.0
@@ -59,6 +56,11 @@
         attended + own_prob.astype(jnp.float32)[..., None] * lat_new.astype(jnp.float32)[:, None, :]
     )
     return attended.astype(jnp.bfloat16)
+
+
+def to_sequences(rows, tp_size, seq_count):
+    blocks = rows.reshape(tp_size, seq_count, rows.shape[1])
+    return lax.all_to_all(blocks, "tp", split_axis=0, concat_axis=0, tiled=True)
 
 
 def on_device(
@@ -97,11 +99,12 @@
     latent_cols = jnp.dot(normed, w_latent_down, preferred_element_type=jnp.float32).astype(
         jnp.bfloat16
     )
-    q_mine, rot_mine, latent_raw = (
-        lax.all_to_all(q_latent, "tp", split_axis=0, concat_axis=1, tiled=True),
-        lax.all_to_all(q_rot, "tp", split_axis=0, concat_axis=1, tiled=True),
-        lax.all_to_all(latent_cols, "tp", split_axis=0, concat_axis=1, tiled=True),
-    )
+    q_cols, rot_cols = q_latent.shape[1], q_rot.shape[1]
+    packed = jnp.concatenate([q_latent, q_rot, latent_cols], axis=1)
+    packed = to_sequences(packed, tp_size, seq_count)
+    q_mine = packed[:, :, :q_cols].transpose(1, 0, 2).reshape(seq_count, -1)
+    rot_mine = packed[:, :, q_cols : q_cols + rot_cols].transpose(1, 0, 2).reshape(seq_count, -1)
+    latent_raw = packed[:, :, q_cols + rot_cols :].transpose(1, 0, 2).reshape(seq_count, -1)
     heads_all = rot_mine.shape[1] // rope_width
     own_normed = lax.dynamic_slice_in_dim(normed, tp_rank * seq_count, seq_count, 0)
     rope_raw = jnp.dot(own_normed, w_rope_down, preferred_element_type=jnp.float32).astype(
@@ -139,50 +142,32 @@
         .reshape(group_rows, -1)
     )
     head_term = jnp.dot(values, w_output, preferred_element_type=jnp.float32)
-    mixed = lax.psum(head_term.astype(jnp.bfloat16), "tp").astype(jnp.float32)
-    resid = (tokens.astype(jnp.float32) + rms_scale(mixed, norm_gains[1])).astype(jnp.bfloat16)
-    expert_in = rms_scale(resid, norm_gains[2]).astype(jnp.bfloat16)
-    own_resid = lax.dynamic_slice_in_dim(resid, tp_rank * seq_count, seq_count, 0)
-    ep_size = lax.axis_size("ep")
-    experts = ep_size * EXP_LOCAL
-    local_expert = tp_rank // (tp_size // EXP_LOCAL)
-    route_count = routes.shape[1]
-    capacity = (
-        (group_rows * route_count + experts - 1) // experts
-        + 2
-        + group_rows * route_count // (4 * experts)
-    )
-    slot_count = ep_size * capacity
-    flat_routes = routes.reshape(-1)
-    expert_hits = (flat_routes[:, None] == jnp.arange(experts, dtype=jnp.int32)[None, :]).astype(
-        jnp.int32
-    )
-    slot_rank = jnp.sum((jnp.cumsum(expert_hits, axis=0) - 1) * expert_hits, axis=1)
-    served_here = flat_routes % EXP_LOCAL == local_expert
-    slot_index = jnp.where(served_here, flat_routes // EXP_LOCAL * capacity + slot_rank, -1)
-    slot_picks = (slot_index[:, None] == jnp.arange(slot_count, dtype=jnp.int32)[None, :]).astype(
-        jnp.bfloat16
-    )
-    slot_picks = slot_picks.reshape(group_rows, route_count, slot_count)
-    slot_rows = jnp.sum(slot_picks, axis=1)
-    outgoing = jnp.dot(slot_rows.T, expert_in, preferred_element_type=jnp.float32).astype(
-        jnp.bfloat16
-    )
-    arrived = lax.all_to_all(outgoing, "ep", split_axis=0, concat_axis=0, tiled=True)
+    terms = to_sequences(head_term.astype(jnp.bfloat16), tp_size, seq_count)
+    mixed = jnp.sum(terms.astype(jnp.float32), axis=0)
+    own_tokens = lax.dynamic_slice_in_dim(tokens, tp_rank * seq_count, seq_count, 0)
+    own_resid = (own_tokens.astype(jnp.float32) + rms_scale(mixed, norm_gains[1])).astype(
+        jnp.bfloat16
+    )
+    expert_in = rms_scale(own_resid, norm_gains[2]).astype(jnp.bfloat16)
+    everyone = ("ep", "tp")
+    devices = lax.axis_size("ep") * tp_size
+    copies = jnp.broadcast_to(expert_in[None], (devices,) + expert_in.shape)
+    arrived = lax.all_to_all(copies, everyone, split_axis=0, concat_axis=0, tiled=True)
+    arrived = arrived.reshape(devices * seq_count, -1)
     gate_sum = jnp.dot(arrived, w_gate[0], preferred_element_type=jnp.float32)
     up_sum = jnp.dot(arrived, w_up[0], preferred_element_type=jnp.float32)
     hidden_units = (jax.nn.silu(gate_sum) * up_sum).astype(jnp.bfloat16)
-    expert_out = jnp.dot(hidden_units, w_down[0], preferred_element_type=jnp.float32).astype(
-        jnp.bfloat16
-    )
-    returned = lax.all_to_all(expert_out, "ep", split_axis=0, concat_axis=0, tiled=True)
-    routed_part = jnp.zeros((group_rows, returned.shape[1]), jnp.float32)
-    for route_slot in range(route_count):
-        chosen = jnp.dot(slot_picks[:, route_slot, :], returned, preferred_element_type=jnp.float32)
-        routed_part = routed_part + route_weights[:, route_slot : route_slot + 1] * chosen
-    routed = lax.psum_scatter(
-        routed_part.astype(jnp.bfloat16), "tp", scatter_dimension=0, tiled=True
-    ).astype(jnp.float32)
+    pieces = jnp.dot(hidden_units, w_down[0], preferred_element_type=jnp.float32).astype(
+        jnp.bfloat16
+    )
+    pieces = pieces.reshape(devices, seq_count, -1)
+    returned = lax.all_to_all(pieces, everyone, split_axis=0, concat_axis=0, tiled=True)
+    own_routes = lax.dynamic_slice_in_dim(routes, tp_rank * seq_count, seq_count, 0)
+    own_weights = lax.dynamic_slice_in_dim(route_weights, tp_rank * seq_count, seq_count, 0)
+    holder = jnp.arange(devices, dtype=jnp.int32) // tp_size
+    picks = own_routes[None, :, :] == holder[:, None, None]
+    scale = jnp.sum(jnp.where(picks, own_weights[None], 0.0), axis=-1)
+    routed = jnp.sum(scale[:, :, None] * returned.astype(jnp.float32), axis=0)
     hidden_out = (own_resid.astype(jnp.float32) + rms_scale(routed, norm_gains[3])).astype(
         jnp.bfloat16
     )

time: 213 us -> 92.1 us (0.43)
  waiting for transfers between devices: 122 us -> 11.9 us
  blocking collectives: 12.5 us -> 29.1 us
  between operations: 16.4 us -> 4.4 us
  starting transfers between devices: 19.6 us -> 7.78 us
  matrix products: 21.2 us -> 18.2 us
    psum x1 -> x0, waiting for transfers between devices: 52.6 us -> none  [on_device(): mixed = lax.psum(head_term.astype(jnp.bfloat16), 'tp').astype(jnp.float32)]
    unnamed x3 -> x0, waiting for transfers between devices: 48.9 us -> none
    all_to_all x1 -> x3, blocking collectives: 12.5 us -> 29.1 us  [the longest x1 14.3 us: on_device(): lax.all_to_all(copies, everyone, split_axis=0, concat_axis=0, tiled=True)]
    all_to_all x5 -> x2, starting transfers between devices: 19.5 us -> 7.78 us  [the longest x1 5.2 us: to_sequences(): return lax.all_to_all(blocks, 'tp', split_axis=0, concat_axis=0, tiled=True)]
    all_to_all x5 -> x2, waiting for transfers between devices: 20.6 us -> 11.9 us  [the longest x1 8.91 us: on_device(): lax.all_to_all(pieces, everyone, split_axis=0, concat_axis=0, tiled=True)]
    broadcast_in_dim x0 -> x1, other arithmetic: none -> 2.17 us  [on_device(): copies = jnp.broadcast_to(expert_in[None], (devices,) + expert_in.shape)]
    all_to_all x6 -> x0, local copies, waits for them, and re-layouts: 2.16 us -> none  [the longest x2 0.87 us: on_device(): lax.all_to_all(expert_out, 'ep', split_axis=0, concat_axis=0, tiled=True)]
    reshape x0 -> x4, other arithmetic: none -> 2.16 us  [the longest x3 1.35 us: to_sequences(): blocks = rows.reshape(tp_size, seq_count, rows.shape[1])]
  transfers between devices with their start and end apart: 7 -> 2, of which waited for: 6 -> 2; matrix products, arithmetic and copies ran while one was open for 6% -> 3% of each run, Pallas kernels for 0% -> 0%
where the time goes in v1:
time: 92.1 us; the launch traced here: 91.3 us
  blocking collectives  29.1 us (32%)
  matrix products  18.2 us (20%)
  other arithmetic  13.3 us (14%)
  waiting for transfers between devices  11.9 us (13%)
  starting transfers between devices  7.78 us (8%)
  local copies, waits for them, and re-layouts  6.6 us (7%)
  between operations  4.4 us (5%)
    all_to_all x1, blocking collectives, on_device(): lax.all_to_all(copies, everyone, split_axis=0, concat_axis=0, tiled=True)  14.3 us
    all_to_all x1, waiting for transfers between devices, on_device(): lax.all_to_all(pieces, everyone, split_axis=0, concat_axis=0, tiled=True)  8.91 us
    all_to_all x1, blocking collectives, on_device(): lax.all_to_all(attended.reshape(seq_count, -1), 'tp', split_axis=1, conca...  7.4 us
    all_to_all x1, blocking collectives, to_sequences(): return lax.all_to_all(blocks, 'tp', split_axis=0, concat_axis=0, tiled=True)  7.4 us
    all_to_all x1, starting transfers between devices, to_sequences(): return lax.all_to_all(blocks, 'tp', split_axis=0, concat_axis=0, tiled=True)  5.2 us
    reduce_sum x5, other arithmetic, rms_scale(): jnp.mean(values_f * values_f, axis=-1, keepdims=True) + EPSILON  4.38 us
    dot_general x1, matrix products, on_device(): jnp.einsum('thn,hnc->thc', q_nope, w_key_up, preferred_element_type=jnp.f...  3.07 us
    dot_general x1, matrix products, on_device(): head_term = jnp.dot(values, w_output, preferred_element_type=jnp.float32)  3.05 us
  transfers between devices with their start and end apart: 2, of which 2 were waited for; matrix products, arithmetic and copies ran while one was open for 3% of the time, Pallas kernels for 0%

profile of v1, /device:TPU:0, one launch (start us, length us, event | category | flops | bytes accessed | tf_op | source)
XLA Modules:
  0.0 91.3 jit_solution(3515742608331666923)
XLA Ops:
  0.7 1.0 %slice.33 = f32[1,4096]{1,0:T(1,128)S(1)} slice(f32[4,4096]{1,0:T(4,128)} %param.19), slice={[0:1], [0:4096]} | slice | bytes 32768 | tf_op jit(solution)/shard_map/slice | solution.py:93
  1.7 1.1 %fusion.36 = f32[8]{0:T(128)S(1)} fusion(bf16[8,4096]{1,0:T(8,128)(2,1)} %param.18), kind=kLoop, calls=%fused_computation.39 | loop fusion | flops 98296 | bytes 65568 | tf_op jit(solution)/shard_map/reduce_sum | solution.py:14
  2.7 0.9 %fusion.38 = bf16[8,4096]{1,0:T(8,128)(2,1)S(1)} fusion(bf16[8,4096]{1,0:T(8,128)(2,1)} %param.18, f32[4096]{0:T(1024)S(1)} %bitcast.117, f32[8]{0:T(128)S(1)} %add_rsqrt_fusion), kind=kLoop, calls=%fused_computation.41 | loop fusion | flops 131072 | bytes 147488 | tf_op jit(solution)/shard_map/convert_element_type | solution.py:93
  3.7 2.0 %convolution_convert_fusion.5 = bf16[8,256]{1,0:T(8,128)(2,1)S(1)} fusion(bf16[8,4096]{1,0:T(8,128)(2,1)S(1)} %fusion.38, bf16[4096,256]{1,0:T(8,128)(2,1)} %param.21), kind=kOutput, calls=%fused_computation.24 | convolution fusion | flops 16779264 | bytes 2166784 | tf_op jit(solution)/shard_map/dot_general | solution.py:98
  5.9 3.1 %convolution_convert_fusion.2 = bf16[4,8,1024]{2,1,0:T(8,128)(2,1)S(1)} fusion(bf16[4,128,1024]{2,1,0:T(8,128)(2,1)S(1)} %copy-done.3, bf16[8,4096]{1,0:T(8,128)(2,1)S(1)} %fusion.38, bf16[4096,512]{1,0:T(8,128)(2,1)} %param.20), kind=kOutput, calls=%fused_computation.17 | convolution fusion | flops 41979904 | bytes 5373952 | tf_op jit(solution)/shard_map/thn,hnc->thc/dot_general | solution.py:96
  9.5 0.7 reduce.25
  10.2 0.8 reshape.457
  11.0 5.2 %all-to-all-start = ((bf16[8,2,2240]{2,1,0:T(2,128)(2,1)}), bf16[8,2,2240]{2,1,0:T(2,128)(2,1)S(1)}, u32[]{:S(2)}, u32[]{:S(2)}) async-start(bf16[8,2,2240]{2,1,0:T(2,128)(2,1)} %reshape.457), calls=%async_computation | async-start | bytes 147456 | tf_op jit(solution)/shard_map/all_to_all | solution.py:63
  16.9 1.3 %fusion.30 = f32[1,64]{1,0:T(1,128)S(1)} fusion(bf16[4096,64]{0,1:T(8,128)(2,1)} %param.27, bf16[8,4096]{1,0:T(8,128)(2,1)S(1)} %fusion.38, s32[]{:T(128)S(6)} %select_n.36), kind=kOutput, calls=%fused_computation.32 | convolution fusion | flops 524416 | bytes 540932 | tf_op jit(solution)/shard_map/dot_general | solution.py:110
  18.2 3.0 %all-to-all-done = bf16[8,2,2240]{2,1,0:T(2,128)(2,1)S(1)} async-done(((bf16[8,2,2240]{2,1,0:T(2,128)(2,1)}), bf16[8,2,2240]{2,1,0:T(2,128)(2,1)S(1)}, u32[]{:S(2)}, u32[]{:S(2)}) %all-to-all-start) | async-done | bytes 71712 | tf_op jit(solution)/shard_map/all_to_all | solution.py:63
  21.8 0.6 multiply_reduce_fusion.4
  23.3 2.4 %fusion.9 = f32[32,1024]{1,0:T(8,128)S(1)} fusion(bf16[32,1024]{1,0:T(8,128)(2,1)S(1)} %reshape.433, bf16[1,1024,1024]{2,1,0:T(8,128)(2,1)} %param.28), kind=kOutput, calls=%fused_computation.11 | convolution fusion | flops 67108864 | bytes 2293760 | tf_op jit(solution)/shard_map/shc,spc->shp/dot_general | solution.py:36
  27.3 1.0 %reduce.26 = bf16[8,4096]{1,0:T(8,128)(2,1)S(1)} reduce(bf16[8,1,4096]{2,1,0:T(2,128)(2,1)S(1)} %bitcast.114, bf16[]{:T(256)} %broadcast.295), dimensions={1}, to_apply=%bitcast.92.reduce_sub_computation | reduce | bytes 131074
  28.3 7.4 %all_to_all.34 = bf16[8,2,2048]{2,1,0:T(2,128)(2,1)S(1)} all-to-all(bf16[8,2,2048]{2,1,0:T(2,128)(2,1)S(1)} %reshape.459), channel_id=1, replica_groups=mesh['ep'=4,'tp'=8] {'tp'}, dimensions={0} | all-to-all | bytes 131072 | tf_op jit(solution)/shard_map/all_to_all | solution.py:131
  36.2 3.1 %fusion.1 = bf16[8,1,4096]{2,0,1:T(8,128)(2,1)S(1)} fusion(bf16[512,4096]{1,0:T(8,128)(2,1)} %param.24, bf16[8,4,1024]{2,0,1:T(8,128)(2,1)S(1)} %bitcast.115, bf16[4,1024,128]{2,1,0:T(8,128)(2,1)S(1)} %copy-done.4), kind=kOutput, calls=%fused_computation.3 | convolution fusion | flops 41979904 | bytes 5373952 | tf_op jit(solution)/shard_map/dot_general | solution.py:144
  39.2 0.7 reduce.27
  40.0 7.4 %all_to_all.35 = bf16[8,2,2048]{2,1,0:T(2,128)(2,1)S(1)} all-to-all(bf16[8,2,2048]{2,1,0:T(2,128)(2,1)S(1)} %reshape.461), channel_id=1, replica_groups=mesh['ep'=4,'tp'=8] {'tp'}, dimensions={0} | all-to-all | bytes 131072 | tf_op jit(solution)/shard_map/all_to_all | solution.py:63
  47.6 0.6 multiply_reduce_fusion.3
  48.9 1.5 %multiply_reduce_fusion.2 = (f32[]{:T(128)}, bf16[1,4096]{1,0:T(2,128)(2,1)S(1)}) fusion(f32[1,4096]{1,0:T(1,128)S(1)} %bitcast.118, f32[4,4096]{1,0:T(4,128)S(1)} %copy-done.6, bf16[8,4096]{1,0:T(8,128)(2,1)} %param.18, s32[]{:T(128)S(6)} %select_n.36), kind=kLoop, calls=%fused_computation.66 | loop fusion | flops 28671 | bytes 49160 | tf_op jit(solution)/shard_map/reduce_sum | solution.py:14
  51.6 2.2 %reduce.28 = bf16[32,4096]{1,0:T(8,128)(2,1)S(1)} reduce(bf16[32,1,4096]{2,1,0:T(2,128)(2,1)S(1)} %broadcast_in_dim.63, bf16[]{:T(256)} %broadcast.295), dimensions={1}, to_apply=%broadcast_in_dim.63.reduce_sub_computation | reduce | bytes 524290 | tf_op jit(solution)/shard_map/broadcast_in_dim | solution.py:154
  54.0 14.3 %all_to_all.36 = bf16[32,2,2048]{2,1,0:T(2,128)(2,1)S(1)} all-to-all(bf16[32,2,2048]{2,1,0:T(2,128)(2,1)S(1)} %reshape.463), channel_id=1, replica_groups=mesh['ep'=4,'tp'=8] {'ep','tp'}, dimensions={0} | all-to-all | bytes 524288 | tf_op jit(solution)/shard_map/all_to_all | solution.py:155
  68.6 2.1 %fusion.5 = f32[32,256]{1,0:T(8,128)S(1)} fusion(bf16[1,4096,256]{2,1,0:T(8,128)(2,1)} %param.33, bf16[32,1,4096]{2,1,0:T(2,128)(2,1)S(1)} %reshape.464), kind=kOutput, calls=%fused_computation.7 | convolution fusion | flops 67108864 | bytes 2392064 | tf_op jit(solution)/shard_map/dot_general | solution.py:157
  70.8 2.9 %fusion = bf16[32,1,4096]{2,0,1:T(8,128)(2,1)S(1)} fusion(bf16[1,256,4096]{2,1,0:T(8,128)(2,1)S(1)} %copy-done, bf16[1,4096,256]{2,1,0:T(8,128)(2,1)} %param.34, bf16[32,1,4096]{2,1,0:T(2,128)(2,1)S(1)} %reshape.464, f32[32,256]{1,0:T(8,128)S(1)} %fusion.5), kind=kOutput, calls=%fused_computation.1 | convolution fusion | flops 134397952 | bytes 4751360 | tf_op jit(solution)/shard_map/dot_general | solution.py:160
  73.6 0.8 reduce.29
  74.4 0.9 reshape.465
  75.3 2.6 %all-to-all-start.4 = ((bf16[32,2,2048]{2,1,0:T(2,128)(2,1)}), bf16[32,2,2048]{2,1,0:T(2,128)(2,1)S(1)}, u32[]{:S(2)}, u32[]{:S(2)}) async-start(bf16[32,2,2048]{2,1,0:T(2,128)(2,1)} %reshape.465), calls=%async_computation.4 | async-start | bytes 524288 | tf_op jit(solution)/shard_map/all_to_all | solution.py:164
  78.3 0.6 pad_maximum_fusion.3
  79.0 0.6 convert_element_type.165
  79.6 8.9 %all-to-all-done.4 = bf16[32,2,2048]{2,1,0:T(2,128)(2,1)S(1)} async-done(((bf16[32,2,2048]{2,1,0:T(2,128)(2,1)}), bf16[32,2,2048]{2,1,0:T(2,128)(2,1)S(1)}, u32[]{:S(2)}, u32[]{:S(2)}) %all-to-all-start.4) | async-done | bytes 262176 | tf_op jit(solution)/shard_map/all_to_all | solution.py:164
  88.7 0.6 multiply_reduce_fusion
  89.4 0.6 multiply_reduce_fusion.1
  90.7 0.6 add_convert_fusion
  (60 shorter events, 5.6 us)
Async XLA Ops:
  0.6 70.1 %copy-start = (bf16[1,256,4096]{2,1,0:T(8,128)(2,1)S(1)}, bf16[1,256,4096]{2,1,0:T(8,128)(2,1)}, u32[]{:S(2)}) copy-start(bf16[1,256,4096]{2,1,0:T(8,128)(2,1)} %param.35) | copy-start | bytes 6291460
  0.6 5.0 %copy-start.2 = (bf16[4096,128]{1,0:T(8,128)(2,1)S(1)}, bf16[4096,128]{1,0:T(8,128)(2,1)}, u32[]{:S(2)}) copy-start(bf16[4096,128]{1,0:T(8,128)(2,1)} %param.25) | copy-start | bytes 3145732
  0.7 5.3 %copy-start.3 = (bf16[4,128,1024]{2,1,0:T(8,128)(2,1)S(1)}, bf16[4,128,1024]{2,1,0:T(8,128)(2,1)}, u32[]{:S(2)}) copy-start(bf16[4,128,1024]{2,1,0:T(8,128)(2,1)} %param.22) | copy-start | bytes 3145732
  5.9 17.3 %copy-start.7 = (f32[1024]{0:T(1024)S(1)}, f32[1024]{0:T(1024)}, u32[]{:S(2)}) copy-start(f32[1024]{0:T(1024)} %param.26) | copy-start | bytes 12292
  9.0 16.9 %copy-start.5 = (bf16[1,1024,64]{1,2,0:T(8,128)(2,1)S(1)}, bf16[1,1024,64]{1,2,0:T(8,128)(2,1)}, u32[]{:S(2)}) copy-start(bf16[1,1024,64]{1,2,0:T(8,128)(2,1)} %param.29) | copy-start | bytes 393220
  11.0 10.3 %all-to-all-start = ((bf16[8,2,2240]{2,1,0:T(2,128)(2,1)}), bf16[8,2,2240]{2,1,0:T(2,128)(2,1)S(1)}, u32[]{:S(2)}, u32[]{:S(2)}) async-start(bf16[8,2,2240]{2,1,0:T(2,128)(2,1)} %reshape.457), calls=%async_computation | async-start | bytes 147456 | tf_op jit(solution)/shard_map/all_to_all | solution.py:63
  23.2 3.5 %copy-start.1 = (bf16[1,1024,1024]{2,1,0:T(8,128)(2,1)S(1)}, bf16[1,1024,1024]{2,1,0:T(8,128)(2,1)}, u32[]{:S(2)}) copy-start(bf16[1,1024,1024]{2,1,0:T(8,128)(2,1)} %param.28) | copy-start | bytes 6291460
  25.7 10.5 %copy-start.4 = (bf16[4,1024,128]{2,1,0:T(8,128)(2,1)S(1)}, bf16[4,1024,128]{2,1,0:T(8,128)(2,1)}, u32[]{:S(2)}) copy-start(bf16[4,1024,128]{2,1,0:T(8,128)(2,1)} %param.23) | copy-start | bytes 3145732
  36.2 12.7 %copy-start.6 = (f32[4,4096]{1,0:T(4,128)S(1)}, f32[4,4096]{1,0:T(4,128)}, u32[]{:S(2)}) copy-start(f32[4,4096]{1,0:T(4,128)} %param.19) | copy-start | bytes 196612
  70.7 7.2 %copy-start.8 = (f32[8,2]{0,1:T(2,128)S(1)}, f32[8,2]{0,1:T(2,128)}, u32[]{:S(2)}) copy-start(f32[8,2]{0,1:T(2,128)} %param.32) | copy-start | bytes 196
  70.7 7.4 %copy-start.9 = (s32[8,2]{0,1:T(2,128)S(1)}, s32[8,2]{0,1:T(2,128)}, u32[]{:S(2)}) copy-start(s32[8,2]{0,1:T(2,128)} %param.31) | copy-start | bytes 196
  75.3 13.2 %all-to-all-start.4 = ((bf16[32,2,2048]{2,1,0:T(2,128)(2,1)}), bf16[32,2,2048]{2,1,0:T(2,128)(2,1)S(1)}, u32[]{:S(2)}, u32[]{:S(2)}) async-start(bf16[32,2,2048]{2,1,0:T(2,128)(2,1)} %reshape.465), calls=%async_computation.4 | async-start | bytes 524288 | tf_op jit(solution)/shard_map/all_to_all | solution.py:164

commit v2 on v1

--- a/solution.py
+++ b/solution.py
@@ -1,6 +1,11 @@
+import functools
+import math
+
 import jax
 import jax.numpy as jnp
 from jax import lax
+from jax.experimental import pallas as pl
+from jax.experimental.pallas import tpu as pltpu
 from jax.sharding import PartitionSpec as P
 
 EPSILON = 1e-06
@@ -63,7 +68,7 @@
     return lax.all_to_all(blocks, "tp", split_axis=0, concat_axis=0, tiled=True)
 
 
-def on_device(
+def on_device_plain(
     tokens,
     norm_gains,
     w_query,
@@ -174,6 +179,502 @@
     return (hidden_out, new_latent, new_rope)
 
 
+LANES = 128
+BIG = 20 * 10**9
+
+
+def dma_chunks(ref, buffer, count):
+    rows = ref.shape[0] // count
+    return [(ref.at[pl.ds(i * rows, rows)], buffer.at[pl.ds(i * rows, rows)]) for i in range(count)]
+
+
+def lane_chunk(value, index):
+    return value[:, index * LANES : (index + 1) * LANES]
+
+
+def mean_scale(value, count):
+    return lax.rsqrt(jnp.sum(value * value, keepdims=True) / count + EPSILON)
+
+
+def query_kernel(
+    tokens,
+    gains,
+    lengths,
+    w_rope,
+    w_query,
+    w_query_rope,
+    w_latent,
+    w_key,
+    rows,
+    own_tokens,
+    gain_rows,
+    new_rope,
+    table,
+    rope_buf,
+    length_buf,
+    tokens_buf,
+    gains_buf,
+    query_buf,
+    query_rope_buf,
+    latent_buf,
+    key_buf,
+    token_rows,
+    sems,
+):
+    group_rows, width = tokens.shape
+    heads, nope, latent = w_key.shape
+    pieces = width // LANES
+    per_head = latent // LANES
+    block = rows.shape[0] // group_rows
+    query_steps = dma_chunks(w_query, query_buf, 4)
+    key_steps = dma_chunks(w_key, key_buf, heads)
+    rot_steps = dma_chunks(w_query_rope, query_rope_buf, 2)
+    latent_steps = dma_chunks(w_latent, latent_buf, 1)
+    rope_steps = [(w_rope, rope_buf)]
+    first_steps = [(tokens, tokens_buf), (gains, gains_buf), (lengths, length_buf)]
+    copies = [
+        pltpu.make_async_copy(src, dst, sems.at[i])
+        for i, (src, dst) in enumerate(
+            first_steps + query_steps + key_steps + rot_steps + latent_steps + rope_steps
+        )
+    ]
+    for copy in copies:
+        copy.start()
+    pending = iter(copies)
+    rank = lax.axis_index("tp")
+
+    next(pending).wait()
+    next(pending).wait()
+    tokens_f = tokens_buf[...].astype(jnp.float32)
+    gains = gains_buf
+    power = jnp.sum(tokens_f * tokens_f, axis=-1, keepdims=True) / width
+    normed = (tokens_f * lax.rsqrt(power + EPSILON) * gains[0:1, :]).astype(jnp.bfloat16)
+    for k in range(pieces):
+        token_rows[pl.ds(k, group_rows, stride=pieces), :] = lane_chunk(tokens_f, k)
+        gain_rows[pl.ds(k, gains.shape[0], stride=pieces), :] = lane_chunk(gains[...], k)
+    own_tokens[...] = token_rows[pl.ds(pl.multiple_of(rank * pieces, pieces), pieces), :]
+    next(pending).wait()
+    half = LANES // 2
+    lane = lax.broadcasted_iota(jnp.int32, (1, LANES), 1)
+    exponent = (lane % (half // 2)).astype(jnp.float32) * (-math.log(ROTARY_BASE) / (half // 2))
+    angles = length_buf[0].astype(jnp.float32) * jnp.exp(exponent)
+    sine = jnp.sin(angles)
+    table[0:1, :] = jnp.cos(angles)
+    table[1:2, :] = jnp.where(lane % half < half // 2, -sine, sine)
+
+    def project(buffer, steps):
+        depth = width // len(steps)
+        total = None
+        for i in range(len(steps)):
+            next(pending).wait()
+            part = jnp.dot(
+                normed[:, i * depth : (i + 1) * depth],
+                buffer[pl.ds(i * depth, depth), :],
+                preferred_element_type=jnp.float32,
+            )
+            total = part if total is None else total + part
+        return total
+
+    q_nope = project(query_buf, query_steps).astype(jnp.bfloat16)
+    for h in range(heads):
+        next(pending).wait()
+        q_latent = jnp.dot(
+            q_nope[:, h * nope : (h + 1) * nope], key_buf[h], preferred_element_type=jnp.float32
+        )
+        for k in range(per_head):
+            rows[pl.ds(h * per_head + k, group_rows, stride=block), :] = lane_chunk(q_latent, k)
+    q_rot = project(query_rope_buf, rot_steps)
+    low = lax.broadcasted_iota(jnp.int32, (group_rows, LANES), 1) < half
+    base = heads * per_head
+    for h in range(heads):
+        pair = lane_chunk(q_rot, h // 2)
+        turned = pltpu.roll(pair, half, 1)
+        twice = jnp.where(low, pair, turned) if h % 2 == 0 else jnp.where(low, turned, pair)
+        rows[pl.ds(base + h, group_rows, stride=block), :] = twice
+    latent_cols = project(latent_buf, latent_steps)
+    for k in range(base + heads, block):
+        rows[pl.ds(k, group_rows, stride=block), :] = latent_cols
+    next(pending).wait()
+    rope_raw = lax.dot_general(
+        normed, rope_buf[...], (((1,), (1,)), ((), ())), preferred_element_type=jnp.float32
+    )
+    mine = lax.broadcasted_iota(jnp.int32, rope_raw.shape, 0) == rank
+    rope_raw = jnp.sum(jnp.where(mine, rope_raw, 0.0), axis=0, keepdims=True)
+    rope_raw = rope_raw.astype(jnp.bfloat16).astype(jnp.float32)
+    twice = jnp.concatenate([rope_raw, rope_raw], axis=1)
+    turned = twice * table[0:1, :] + pltpu.roll(twice, half // 2, 1) * table[1:2, :]
+    new_rope[...] = turned[:, :half].astype(jnp.bfloat16)
+
+
+def pack_kernel(rows, send):
+    block = send.shape[1]
+    for j in range(send.shape[0]):
+        send[j] = rows[pl.ds(j * block, block), :].astype(jnp.bfloat16)
+
+
+def attend_kernel(
+    length,
+    received,
+    cache,
+    cache_rope,
+    table,
+    gain,
+    rope_new,
+    send,
+    new_latent,
+    rows,
+    extra,
+    rot_rows,
+    queries,
+    score_scale,
+):
+    sources, block, _ = received.shape
+    latent = cache.shape[1]
+    per_head = latent // LANES
+    rope = cache_rope.shape[0]
+    heads = queries.shape[0]
+    here = heads // sources
+    base = here * per_head
+    tail = block - base
+    for j in range(sources):
+        piece = received[j].astype(jnp.float32)
+        rows[pl.ds(j * base, base), :] = piece[:base]
+        extra[pl.ds(j * tail, tail), :] = piece[base:]
+    for k in range(per_head):
+        queries[:, k * LANES : (k + 1) * LANES] = rows[
+            pl.ds(k, heads, stride=per_head), :
+        ].astype(jnp.bfloat16)
+    for j in range(sources):
+        rot_rows[pl.ds(j * here, here), :] = extra[pl.ds(j * tail, here), :]
+    latent_raw = extra[pl.ds(here, sources, stride=tail), :]
+    latent_f = (latent_raw * mean_scale(latent_raw, latent) * gain[...]).astype(jnp.bfloat16)
+    latent_f = latent_f.astype(jnp.float32)
+    for k in range(per_head):
+        new_latent[:, k * LANES : (k + 1) * LANES] = latent_f[k : k + 1, :].astype(jnp.bfloat16)
+    rot = rot_rows[...]
+    q_pe = rot * table[0:1, :] + pltpu.roll(rot, LANES // 4, 1) * table[1:2, :]
+    q_pe = q_pe[:, :rope].astype(jnp.bfloat16)
+    q = queries[...]
+    scores = lax.dot_general(
+        q, cache[...], (((1,), (1,)), ((), ())), preferred_element_type=jnp.float32
+    )
+    scores = scores + jnp.dot(q_pe, cache_rope[...], preferred_element_type=jnp.float32)
+    scores = scores * score_scale
+    q_f = q.astype(jnp.float32)
+    products = lane_chunk(q_f, 0) * latent_f[0:1, :]
+    for k in range(1, per_head):
+        products = products + lane_chunk(q_f, k) * latent_f[k : k + 1, :]
+    own = jnp.sum(products, axis=1, keepdims=True)
+    own = own + jnp.sum(
+        q_pe.astype(jnp.float32) * rope_new[...].astype(jnp.float32), axis=1, keepdims=True
+    )
+    own = own * score_scale
+    visible = lax.broadcasted_iota(jnp.int32, scores.shape, 1) < length[0]
+    top = jnp.maximum(jnp.max(jnp.where(visible, scores, -jnp.inf), axis=1, keepdims=True), own)
+    weights = jnp.where(visible, jnp.exp(scores - top), 0.0)
+    own_weight = jnp.exp(own - top)
+    total = jnp.sum(weights, axis=1, keepdims=True) + own_weight
+    probs = (weights / total).astype(jnp.bfloat16)
+    own_prob = (own_weight / total).astype(jnp.bfloat16).astype(jnp.float32)
+    attended = jnp.dot(probs, cache[...], preferred_element_type=jnp.float32)
+    for k in range(per_head):
+        rows[pl.ds(k, heads, stride=per_head), :] = (
+            lane_chunk(attended, k) + own_prob * latent_f[k : k + 1, :]
+        )
+    for j in range(sources):
+        send[j] = rows[pl.ds(j * base, base), :].astype(jnp.bfloat16)
+
+
+def output_kernel(received, w_value, w_output, send, rows, term_rows):
+    sources, block, _ = received.shape
+    heads, latent, _ = w_value.shape
+    per_head = latent // LANES
+    pieces = w_output.shape[1] // LANES
+    for j in range(sources):
+        rows[pl.ds(j * block, block), :] = received[j].astype(jnp.float32)
+    values = []
+    for h in range(heads):
+        attended = jnp.concatenate(
+            [
+                rows[pl.ds(h * per_head + k, sources, stride=block), :].astype(jnp.bfloat16)
+                for k in range(per_head)
+            ],
+            axis=1,
+        )
+        values.append(
+            jnp.dot(attended, w_value[h], preferred_element_type=jnp.float32).astype(jnp.bfloat16)
+        )
+    values = jnp.concatenate(values, axis=1)
+    step = 4
+    for c in range(0, pieces, step):
+        term = jnp.dot(
+            values,
+            w_output[:, c * LANES : (c + step) * LANES],
+            preferred_element_type=jnp.float32,
+        )
+        for k in range(step):
+            term_rows[pl.ds(c + k, sources, stride=pieces), :] = lane_chunk(term, k)
+    for j in range(sources):
+        send[j] = term_rows[pl.ds(j * pieces, pieces), :].astype(jnp.bfloat16)
+
+
+def resid_kernel(routes, route_weights, received, own_tokens, gain_rows, send, resid, scales):
+    mine = lax.broadcasted_iota(jnp.int32, routes.shape, 1) == lax.axis_index("tp")
+    named = jnp.sum(jnp.where(mine, routes[...], 0), axis=1, keepdims=True)
+    weight = jnp.sum(jnp.where(mine, route_weights[...], 0.0), axis=1, keepdims=True)
+    for e in range(scales.shape[0]):
+        total = jnp.sum(jnp.where(named == e, weight, 0.0), axis=0, keepdims=True)
+        scales[e : e + 1, :] = jnp.broadcast_to(total, (1, LANES))
+    pieces = received.shape[1]
+    count = pieces * LANES
+    mixed = received[0].astype(jnp.float32)
+    for j in range(1, received.shape[0]):
+        mixed = mixed + received[j].astype(jnp.float32)
+    after = own_tokens[...] + mixed * mean_scale(mixed, count) * gain_rows[pieces : 2 * pieces]
+    after = after.astype(jnp.bfloat16).astype(jnp.float32)
+    resid[...] = after
+    expert_in = after * mean_scale(after, count) * gain_rows[2 * pieces : 3 * pieces]
+    expert_in = expert_in.astype(jnp.bfloat16)
+    for j in range(send.shape[0]):
+        send[j] = expert_in
+
+
+def expert_kernel(received, w_gate, w_up, w_down, send, rows, inputs):
+    sources, pieces, _ = received.shape
+    for j in range(sources):
+        rows[pl.ds(j * pieces, pieces), :] = received[j].astype(jnp.float32)
+    for k in range(pieces):
+        inputs[:, k * LANES : (k + 1) * LANES] = rows[
+            pl.ds(k, sources, stride=pieces), :
+        ].astype(jnp.bfloat16)
+    gate = jnp.dot(inputs[...], w_gate[...], preferred_element_type=jnp.float32)
+    up = jnp.dot(inputs[...], w_up[...], preferred_element_type=jnp.float32)
+    inner = (gate / (1.0 + jnp.exp(-gate)) * up).astype(jnp.bfloat16)
+    step = 4
+    for c in range(0, pieces, step):
+        piece = jnp.dot(
+            inner, w_down[:, c * LANES : (c + step) * LANES], preferred_element_type=jnp.float32
+        )
+        for k in range(step):
+            rows[pl.ds(c + k, sources, stride=pieces), :] = lane_chunk(piece, k)
+    for j in range(sources):
+        send[j] = rows[pl.ds(j * pieces, pieces), :].astype(jnp.bfloat16)
+
+
+def final_kernel(scales, received, resid, gain_rows, hidden):
+    sources, pieces, _ = received.shape
+    experts = scales.shape[0]
+    per_expert = sources // experts
+    routed = None
+    for e in range(experts):
+        block = received[e * per_expert].astype(jnp.float32)
+        for b in range(1, per_expert):
+            block = block + received[e * per_expert + b].astype(jnp.float32)
+        part = block * scales[e : e + 1, :]
+        routed = part if routed is None else routed + part
+    out = resid[...] + routed * mean_scale(routed, pieces * LANES) * gain_rows[3 * pieces :]
+    for k in range(pieces):
+        hidden[:, k * LANES : (k + 1) * LANES] = out[k : k + 1, :].astype(jnp.bfloat16)
+
+
+def kernel_call(body, outs, specs, scratch, megabytes, flops, name):
+    bytes_moved = 32 * 1024 * 1024 if flops >= BIG else 4 * 1024 * 1024
+    return pl.pallas_call(
+        body,
+        out_shape=outs,
+        in_specs=specs,
+        out_specs=jax.tree.map(lambda _: pl.BlockSpec(memory_space=pltpu.VMEM), outs),
+        scratch_shapes=scratch,
+        compiler_params=pltpu.CompilerParams(vmem_limit_bytes=megabytes * 1024 * 1024),
+        cost_estimate=pl.CostEstimate(
+            flops=flops, bytes_accessed=bytes_moved, transcendentals=0
+        ),
+        name=name,
+    )
+
+
+def lanes_fit(w_key_up, w_value_up, w_latent_down, w_rope_down, cache_latent, tp_size):
+    return (
+        cache_latent.shape[0] == 1
+        and w_latent_down.shape[1] == LANES
+        and w_key_up.shape[0] % 2 == 0
+        and w_key_up.shape[1] == LANES
+        and w_value_up.shape[2] == LANES
+        and 2 * w_rope_down.shape[1] == LANES
+        and w_key_up.shape[2] == tp_size * LANES
+        and w_key_up.shape[0] * w_key_up.shape[2] // LANES % 8 == 0
+        and w_key_up.shape[0] < 8
+    )
+
+
+def on_device_fused(
+    tokens,
+    norm_gains,
+    w_query,
+    w_query_rope,
+    w_key_up,
+    w_value_up,
+    w_output,
+    w_latent_down,
+    latent_gain,
+    w_rope_down,
+    cache_latent,
+    cache_rope,
+    lengths,
+    routes,
+    route_weights,
+    w_gate,
+    w_up,
+    w_down,
+):
+    tp_size = lax.axis_size("tp")
+    ep_size = lax.axis_size("ep")
+    devices = tp_size * ep_size
+    heads_here, nope, latent = w_key_up.shape
+    heads = heads_here * tp_size
+    group_rows, width = tokens.shape
+    rope = w_rope_down.shape[1]
+    cached = cache_latent.shape[1]
+    pieces = width // LANES
+    per_head = latent // LANES
+    base = heads_here * per_head
+    block = base + 8
+    bf16, f32 = jnp.bfloat16, jnp.float32
+    vmem = pl.BlockSpec(memory_space=pltpu.VMEM)
+    smem = pl.BlockSpec(memory_space=pltpu.SMEM)
+    hbm = pl.BlockSpec(memory_space=pltpu.HBM)
+    shape = jax.ShapeDtypeStruct
+
+    rows, own_tokens, gain_rows, new_rope, table = kernel_call(
+        query_kernel,
+        (
+            shape((group_rows * block, LANES), f32),
+            shape((pieces, LANES), f32),
+            shape((norm_gains.shape[0] * pieces, LANES), f32),
+            shape((1, rope), bf16),
+            shape((2, LANES), f32),
+        ),
+        [hbm] * 8,
+        [
+            pltpu.VMEM((rope, width), bf16),
+            pltpu.SMEM(lengths.shape, jnp.int32),
+            pltpu.VMEM(tokens.shape, bf16),
+            pltpu.VMEM(norm_gains.shape, f32),
+            pltpu.VMEM(w_query.shape, bf16),
+            pltpu.VMEM(w_query_rope.shape, bf16),
+            pltpu.VMEM(w_latent_down.shape, bf16),
+            pltpu.VMEM(w_key_up.shape, bf16),
+            pltpu.VMEM((group_rows * pieces, LANES), f32),
+            pltpu.SemaphoreType.DMA((11 + heads_here,)),
+        ],
+        61,
+        2 * group_rows * w_query.size,
+        "queries",
+    )(
+        tokens,
+        norm_gains,
+        lengths,
+        w_rope_down.T,
+        w_query,
+        w_query_rope,
+        w_latent_down,
+        w_key_up,
+    )
+    send = kernel_call(
+        pack_kernel,
+        shape((tp_size, block, LANES), bf16),
+        [vmem],
+        [],
+        2,
+        BIG,
+        "pack",
+    )(rows)
+    received = lax.all_to_all(send, "tp", split_axis=0, concat_axis=0, tiled=True)
+    send, new_latent = kernel_call(
+        functools.partial(attend_kernel, score_scale=(nope + rope) ** (-0.5)),
+        (shape((tp_size, base, LANES), bf16), shape((1, latent), bf16)),
+        [smem] + [vmem] * 6,
+        [
+            pltpu.VMEM((tp_size * base, LANES), f32),
+            pltpu.VMEM((tp_size * 8, LANES), f32),
+            pltpu.VMEM((heads, LANES), f32),
+            pltpu.VMEM((heads, latent), bf16),
+        ],
+        8,
+        4 * heads * cached * latent,
+        "attend",
+    )(
+        lengths,
+        received,
+        cache_latent[0],
+        cache_rope[0].T,
+        table,
+        latent_gain.reshape(-1, LANES),
+        new_rope,
+    )
+    received = lax.all_to_all(send, "tp", split_axis=0, concat_axis=0, tiled=True)
+    send = kernel_call(
+        output_kernel,
+        shape((tp_size, pieces, LANES), bf16),
+        [vmem] * 3,
+        [
+            pltpu.VMEM((tp_size * base, LANES), f32),
+            pltpu.VMEM((tp_size * pieces, LANES), f32),
+        ],
+        10,
+        2 * group_rows * (w_output.size + w_value_up.size),
+        "outputs",
+    )(received, w_value_up, w_output)
+    received = lax.all_to_all(send, "tp", split_axis=0, concat_axis=0, tiled=True)
+    send, resid, scales = kernel_call(
+        resid_kernel,
+        (
+            shape((devices, pieces, LANES), bf16),
+            shape((pieces, LANES), f32),
+            shape((ep_size, LANES), f32),
+        ),
+        [vmem] * 5,
+        [],
+        4,
+        10 * tp_size * width,
+        "resid",
+    )(routes.T, route_weights.T, received, own_tokens, gain_rows)
+    everyone = ("ep", "tp")
+    received = lax.all_to_all(send, everyone, split_axis=0, concat_axis=0, tiled=True)
+    send = kernel_call(
+        expert_kernel,
+        shape((devices, pieces, LANES), bf16),
+        [vmem] * 4,
+        [
+            pltpu.VMEM((devices * pieces, LANES), f32),
+            pltpu.VMEM((devices, width), bf16),
+        ],
+        12,
+        6 * devices * w_gate.size,
+        "experts",
+    )(received, w_gate[0], w_up[0], w_down[0])
+    received = lax.all_to_all(send, everyone, split_axis=0, concat_axis=0, tiled=True)
+    hidden = kernel_call(
+        final_kernel,
+        shape((1, width), bf16),
+        [vmem] * 4,
+        [],
+        4,
+        2 * devices * width,
+        "final",
+    )(scales, received, resid, gain_rows)
+    return hidden, new_latent, new_rope
+
+
+def on_device(*arrays):
+    w_key_up, w_value_up, w_latent_down, w_rope_down = (arrays[i] for i in (4, 5, 7, 9))
+    if lanes_fit(
+        w_key_up, w_value_up, w_latent_down, w_rope_down, arrays[10], lax.axis_size("tp")
+    ):
+        return on_device_fused(*arrays)
+    return on_device_plain(*arrays)
+
+
 def solution(mesh):
     in_specs = (
         P("ep", None),

time: 92.1 us -> 65.7 us (0.71)
  blocking collectives: 29.1 us -> 52.5 us
  matrix products: 18.2 us -> 0 us
  other arithmetic: 13.3 us -> 0 us
  waiting for transfers between devices: 11.9 us -> 0 us
  Pallas kernels: 0 us -> 10.4 us
  starting transfers between devices: 7.78 us -> 0 us
  local copies, waits for them, and re-layouts: 6.6 us -> 0.98 us
  between operations: 4.4 us -> 1.45 us
    all_to_all x3 -> x5, blocking collectives: 29.1 us -> 52.5 us  [the longest x2 27.1 us: on_device_fused(): lax.all_to_all(send, everyone, split_axis=0, concat_axis=0, tiled=True)]
    dot_general x12 -> x0, matrix products: 18.2 us -> none  [the longest x1 3.07 us: on_device(): jnp.einsum('thn,hnc->thc', q_nope, w_key_up, preferred_element_type=jnp.f...]
    all_to_all x2 -> x0, waiting for transfers between devices: 11.9 us -> none  [the longest x1 8.91 us: on_device(): lax.all_to_all(pieces, everyone, split_axis=0, concat_axis=0, tiled=True)]
    pallas_call x0 -> x7, Pallas kernels: none -> 10.4 us  [the longest x1 5.53 us: on_device_fused(): kernel_call(query_kernel, (shape((group_rows * block, LANES), f32), shape...]
    all_to_all x2 -> x0, starting transfers between devices: 7.78 us -> none  [the longest x1 5.2 us: to_sequences(): return lax.all_to_all(blocks, 'tp', split_axis=0, concat_axis=0, tiled=True)]
    reduce_sum x9 -> x0, other arithmetic: 5.45 us -> none  [the longest x5 4.38 us: rms_scale(): jnp.mean(values_f * values_f, axis=-1, keepdims=True) + EPSILON]
    broadcast_in_dim x1 -> x0, other arithmetic: 2.17 us -> none  [on_device(): copies = jnp.broadcast_to(expert_in[None], (devices,) + expert_in.shape)]
    reshape x4 -> x0, other arithmetic: 2.16 us -> none  [the longest x3 1.35 us: to_sequences(): blocks = rows.reshape(tp_size, seq_count, rows.shape[1])]
  transfers between devices with their start and end apart: 2 -> 0, of which waited for: 2 -> 0; matrix products, arithmetic and copies ran while one was open for 3% -> 0% of each run, Pallas kernels for 0% -> 0%
where the time goes in v2:
time: 65.7 us; the launch traced here: 65.4 us
  blocking collectives  52.5 us (80%)
  Pallas kernels  10.4 us (16%)
  between operations  1.45 us (2%)
  local copies, waits for them, and re-layouts  0.98 us (1%)
    all_to_all x2, blocking collectives, on_device_fused(): lax.all_to_all(send, everyone, split_axis=0, concat_axis=0, tiled=True)  27.1 us
    all_to_all x3, blocking collectives, on_device_fused(): lax.all_to_all(send, 'tp', split_axis=0, concat_axis=0, tiled=True)  25.4 us
    pallas_call x1, Pallas kernels, on_device_fused(): kernel_call(query_kernel, (shape((group_rows * block, LANES), f32), shape...  5.53 us
    pallas_call x1, Pallas kernels, on_device_fused(): kernel_call(functools.partial(attend_kernel, score_scale=(nope + rope) **...  1.47 us
    pallas_call x1, Pallas kernels, on_device_fused(): kernel_call(expert_kernel, shape((devices, pieces, LANES), bf16), [vmem]...  1.41 us

profile of v2, /device:TPU:0, one launch (start us, length us, event | category | flops | bytes accessed | tf_op | source)
XLA Modules:
  0.0 65.4 jit_solution(14958532159788835280)
XLA Ops:
  1.3 5.5 %queries.1 = (f32[320,128]{1,0:T(8,128)}, f32[32,128]{1,0:T(8,128)}, f32[128,128]{1,0:T(8,128)}, bf16[1,64]{1,0:T(2,128)(2,1)}, f32[2,128]{1,0:T(2,128)}) custom-call(bf16[8,4096]{1,0:T(8,128)(2,1)} %tokens.1, f32[4,4096]{1,0:T(4,128)} %gains.1, s32[1]{0:T(128)S(6)} %copy.21.lengths.length, bf16[64,4096]{1,0:T(8,128)(2,1)} %bitcast.19, ...), custom_call_target="tpu_custom_call" | custom-call | flops 33554432 | bytes 4194304 | tf_op jit(solution)/shard_map/queries/pallas_call | solution.py:548
  6.8 0.0 copy-start.14
  6.8 0.9 %copy-done.14 = f32[320,128]{1,0:T(8,128)S(1)} copy-done((f32[320,128]{1,0:T(8,128)S(1)}, f32[320,128]{1,0:T(8,128)}, u32[]{:S(2)}) %copy-start.14) | copy-done | bytes 163864
  7.7 0.0 copy-start.13
  7.8 0.0 copy-start
  7.8 0.0 copy-start.5
  7.8 10.4 %all_to_all.25.received = bf16[8,40,128]{2,1,0:T(8,128)(2,1)S(1)} all-to-all(bf16[8,40,128]{2,1,0:T(8,128)(2,1)S(1)} %pack.1), channel_id=1, replica_groups=mesh['ep'=4,'tp'=8] {'tp'}, dimensions={0} | all-to-all | bytes 163840 | tf_op jit(solution)/shard_map/all_to_all | solution.py:592
  18.2 0.0 copy-done.1
  18.2 0.0 copy-done.7
  18.2 0.0 copy-done.9
  18.2 0.0 copy-done.12
  18.2 0.0 copy-done.13
  18.2 0.0 copy-start.6
  18.2 0.0 copy-start.8
  18.2 0.0 copy-start.10
  18.2 0.0 copy-start.11
  18.2 1.5 %attend.1 = (bf16[8,32,128]{2,1,0:T(8,128)(2,1)S(1)}, bf16[1,1024]{1,0:T(2,128)(2,1)}) custom-call(s32[1]{0:T(128)S(6)} %copy.21.lengths.length, bf16[8,40,128]{2,1,0:T(8,128)(2,1)S(1)} %all_to_all.25.received, bf16[1024,1024]{1,0:T(8,128)(2,1)S(1)} %bitcast.11, bf16[64,1024]{1,0:T(8,128)(2,1)S(1)} %bitcast.15, f32[2,128]{1,0:T(2,128)S(1)} %copy-done.12, ...), custom_call_target="tpu_custom_call" | custom-call | flops 134217728 | bytes 4194304 | tf_op jit(solution)/shard_map/attend/pallas_call | solution.py:593
  19.7 0.0 copy-start.4
  19.7 7.5 %all_to_all.26.received = bf16[8,32,128]{2,1,0:T(8,128)(2,1)S(1)} all-to-all(bf16[8,32,128]{2,1,0:T(8,128)(2,1)S(1)} %get-tuple-element.16), channel_id=1, replica_groups=mesh['ep'=4,'tp'=8] {'tp'}, dimensions={0} | all-to-all | bytes 131072 | tf_op jit(solution)/shard_map/all_to_all | solution.py:615
  27.3 0.0 copy-done
  27.3 0.0 copy-done.5
  27.3 0.9 %outputs.1 = bf16[8,32,128]{2,1,0:T(8,128)(2,1)S(1)} custom-call(bf16[8,32,128]{2,1,0:T(8,128)(2,1)S(1)} %all_to_all.26.received, bf16[4,1024,128]{2,1,0:T(8,128)(2,1)S(1)} %copy-done.5, bf16[512,4096]{1,0:T(8,128)(2,1)S(1)} %copy-done), custom_call_target="tpu_custom_call" | custom-call | flops 41943040 | bytes 4194304 | tf_op jit(solution)/shard_map/outputs/pallas_call | solution.py:616
  28.2 7.5 %all_to_all.27.received = bf16[8,32,128]{2,1,0:T(8,128)(2,1)S(1)} all-to-all(bf16[8,32,128]{2,1,0:T(8,128)(2,1)S(1)} %outputs.1), channel_id=1, replica_groups=mesh['ep'=4,'tp'=8] {'tp'}, dimensions={0} | all-to-all | bytes 131072 | tf_op jit(solution)/shard_map/all_to_all | solution.py:628
  35.7 0.0 copy-done.6
  35.7 0.0 copy-done.8
  35.7 0.0 copy-done.10
  35.7 0.3 resid.1
  36.0 14.3 %all_to_all.28.received = bf16[32,32,128]{2,1,0:T(8,128)(2,1)S(1)} all-to-all(bf16[32,32,128]{2,1,0:T(8,128)(2,1)S(1)} %get-tuple-element.20), channel_id=1, replica_groups=mesh['ep'=4,'tp'=8] {'ep','tp'}, dimensions={0} | all-to-all | bytes 524288 | tf_op jit(solution)/shard_map/all_to_all | solution.py:643
  50.4 0.0 copy-done.4
  50.4 1.4 %experts.1 = bf16[32,32,128]{2,1,0:T(8,128)(2,1)S(1)} custom-call(bf16[32,32,128]{2,1,0:T(8,128)(2,1)S(1)} %all_to_all.28.received, bf16[4096,256]{1,0:T(8,128)(2,1)S(1)} %bitcast.12, bf16[4096,256]{1,0:T(8,128)(2,1)S(1)} %bitcast.13, bf16[256,4096]{1,0:T(8,128)(2,1)S(1)} %bitcast.14), custom_call_target="tpu_custom_call" | custom-call | flops 201326592 | bytes 4194304 | tf_op jit(solution)/shard_map/experts/pallas_call | solution.py:644
  51.8 12.8 %all_to_all.29.received = bf16[32,32,128]{2,1,0:T(8,128)(2,1)S(1)} all-to-all(bf16[32,32,128]{2,1,0:T(8,128)(2,1)S(1)} %experts.1), channel_id=1, replica_groups=mesh['ep'=4,'tp'=8] {'ep','tp'}, dimensions={0} | all-to-all | bytes 524288 | tf_op jit(solution)/shard_map/all_to_all | solution.py:656
  64.6 0.8 %final.1 = bf16[1,4096]{1,0:T(2,128)(2,1)} custom-call(f32[4,128]{1,0:T(4,128)S(1)} %get-tuple-element.19.scales, bf16[32,32,128]{2,1,0:T(8,128)(2,1)S(1)} %all_to_all.29.received, f32[32,128]{1,0:T(8,128)S(1)} %get-tuple-element.21.resid, f32[128,128]{1,0:T(8,128)S(1)} %copy-done.6), custom_call_target="tpu_custom_call" | custom-call | flops 262144 | bytes 4194304 | tf_op jit(solution)/shard_map/final/pallas_call | solution.py:657
  (10 shorter events, 0.0 us)
Async XLA Ops:
  6.8 0.9 %copy-start.14 = (f32[320,128]{1,0:T(8,128)S(1)}, f32[320,128]{1,0:T(8,128)}, u32[]{:S(2)}) copy-start(f32[320,128]{1,0:T(8,128)} %get-tuple-element.13.rows) | copy-start | bytes 491524
  7.7 10.4 %copy-start.1 = (bf16[1,1024,1024]{2,1,0:T(8,128)(2,1)S(1)}, bf16[1,1024,1024]{2,1,0:T(8,128)(2,1)}, u32[]{:S(2)}) copy-start(bf16[1,1024,1024]{2,1,0:T(8,128)(2,1)} %param.28) | copy-start | bytes 6291460
  7.7 10.4 %copy-start.7 = (bf16[1,1024,64]{1,2,0:T(8,128)(2,1)S(1)}, bf16[1,1024,64]{1,2,0:T(8,128)(2,1)}, u32[]{:S(2)}) copy-start(bf16[1,1024,64]{1,2,0:T(8,128)(2,1)} %param.29) | copy-start | bytes 393220
  7.7 10.4 %copy-start.9 = (f32[1024]{0:T(1024)S(1)}, f32[1024]{0:T(1024)}, u32[]{:S(2)}) copy-start(f32[1024]{0:T(1024)} %param.26) | copy-start | bytes 12292
  7.7 10.4 %copy-start.12 = (f32[2,128]{1,0:T(2,128)S(1)}, f32[2,128]{1,0:T(2,128)}, u32[]{:S(2)}) copy-start(f32[2,128]{1,0:T(2,128)} %get-tuple-element.14.table) | copy-start | bytes 3076
  7.7 10.4 %copy-start.13 = (bf16[1,64]{1,0:T(2,128)(2,1)S(1)}, bf16[1,64]{1,0:T(2,128)(2,1)}, u32[]{:S(2)}) copy-start(bf16[1,64]{1,0:T(2,128)(2,1)} %get-tuple-element.12.rope_new) | copy-start | bytes 388
  7.8 19.5 %copy-start = (bf16[512,4096]{1,0:T(8,128)(2,1)S(1)}, bf16[512,4096]{1,0:T(8,128)(2,1)}, u32[]{:S(2)}) copy-start(bf16[512,4096]{1,0:T(8,128)(2,1)} %w_output.1) | copy-start | bytes 12582916
  7.8 19.5 %copy-start.5 = (bf16[4,1024,128]{2,1,0:T(8,128)(2,1)S(1)}, bf16[4,1024,128]{2,1,0:T(8,128)(2,1)}, u32[]{:S(2)}) copy-start(bf16[4,1024,128]{2,1,0:T(8,128)(2,1)} %w_value.1) | copy-start | bytes 3145732
  18.2 17.5 %copy-start.6 = (f32[128,128]{1,0:T(8,128)S(1)}, f32[128,128]{1,0:T(8,128)}, u32[]{:S(2)}) copy-start(f32[128,128]{1,0:T(8,128)} %get-tuple-element.18.gain_rows) | copy-start | bytes 196612
  18.2 17.5 %copy-start.8 = (f32[32,128]{1,0:T(8,128)S(1)}, f32[32,128]{1,0:T(8,128)}, u32[]{:S(2)}) copy-start(f32[32,128]{1,0:T(8,128)} %get-tuple-element.17.own_tokens) | copy-start | bytes 49156
  18.2 17.5 %copy-start.10 = (s32[8,2]{0,1:T(2,128)S(1)}, s32[8,2]{0,1:T(2,128)}, u32[]{:S(2)}) copy-start(s32[8,2]{0,1:T(2,128)} %param.31) | copy-start | bytes 196
  18.2 17.5 %copy-start.11 = (f32[8,2]{0,1:T(2,128)S(1)}, f32[8,2]{0,1:T(2,128)}, u32[]{:S(2)}) copy-start(f32[8,2]{0,1:T(2,128)} %param.32) | copy-start | bytes 196
  19.7 30.7 %copy-start.4 = (bf16[1,256,4096]{2,1,0:T(8,128)(2,1)S(1)}, bf16[1,256,4096]{2,1,0:T(8,128)(2,1)}, u32[]{:S(2)}) copy-start(bf16[1,256,4096]{2,1,0:T(8,128)(2,1)} %param.35) | copy-start | bytes 6291460
  27.3 23.1 %copy-start.2 = (bf16[1,4096,256]{2,1,0:T(8,128)(2,1)S(1)}, bf16[1,4096,256]{2,1,0:T(8,128)(2,1)}, u32[]{:S(2)}) copy-start(bf16[1,4096,256]{2,1,0:T(8,128)(2,1)} %param.33) | copy-start | bytes 6291460
  27.3 23.1 %copy-start.3 = (bf16[1,4096,256]{2,1,0:T(8,128)(2,1)S(1)}, bf16[1,4096,256]{2,1,0:T(8,128)(2,1)}, u32[]{:S(2)}) copy-start(bf16[1,4096,256]{2,1,0:T(8,128)(2,1)} %param.34) | copy-start | bytes 6291460
